TPU v7x, 32 devices: a whole 2x2x4 slice. The times are simulated.
32 devices in a mesh: sp: 8 (over z, y), tp: 4 (over x, core).
Axes of the slice: x: 2, y: 2, z: 4, core: 2. Of those that a mesh axis runs over, the one named last changes fastest.
Arguments:
- tokens: bfloat16 [4, 512, 1024], P(None, 'sp', 'tp'), may hold values from -6 to 6
- norm_gain: float32 [4, 1024], replicated, may hold values from 0.1 to 1.9
- val_weight: bfloat16 [4, 1024, 512], P(None, 'sp', 'tp'), may hold values from -0.1875 to 0.1875
- gate_weight: bfloat16 [4, 1024, 512], P(None, 'sp', 'tp'), may hold values from -0.1875 to 0.1875
- conv_taps: float32 [4, 31, 512], P(None, None, 'tp'), may hold values from -1 to 1
- conv_bias: float32 [4, 512], P(None, 'tp'), may hold values from -3 to 3
- ln_gain: float32 [4, 512], P(None, 'tp'), may hold values from 0.1 to 1.9
- ln_shift: float32 [4, 512], P(None, 'tp'), may hold values from -3 to 3
- out_weight: bfloat16 [4, 512, 1024], P(None, 'tp', 'sp'), may hold values from -0.25 to 0.25
Outputs:
- stream: bfloat16 [4, 512, 1024], P(None, 'sp', 'tp')
All inputs are finite; a program needn't handle non-finite values.
Results may differ from a plain program's by a relative error of at most 0.02.
Values may be sent and summed in bfloat16 or wider, within the bound.
A program may use at most 64 MiB of HBM per device.

v0:
```python
from functools import partial
import jax
import jax.numpy as jnp
from jax import lax
from jax.sharding import PartitionSpec as P

LAYERS = 4
epsilon = 1e-06


def over_all(shard, axis, dim, absorb, state):
    everything = jax.tree.map(lambda a: lax.all_gather(a, axis, axis=dim, tiled=True), shard)
    return absorb(state, everything, jnp.int32(0))


def with_halo(shard, sides, width, wrap):
    for axis, dim in sides:
        size, length = (lax.axis_size(axis), shard.shape[dim])
        up = [(i, (i + 1) % size) for i in range(size if wrap else size - 1)]
        down = [(j, i) for i, j in up]
        last = lax.slice_in_dim(shard, length - width, length, axis=dim)
        initial = lax.slice_in_dim(shard, 0, width, axis=dim)
        before = lax.ppermute(last, axis, up)
        after = lax.ppermute(initial, axis, down)
        shard = jnp.concatenate([before, shard, after], axis=dim)
    return shard


def over_all_2(shard, axis, dim, work):
    return work(lax.all_gather(shard, axis, axis=dim, tiled=True), jnp.int32(0))


def depthwise(padded, tap_weights, length):
    running = padded[:, 0:length] * tap_weights[0]
    for tap_idx in range(1, tap_weights.shape[0]):
        running = running + padded[:, tap_idx : tap_idx + length] * tap_weights[tap_idx]
    return running


def add_rows(left_rows, running, shard_piece, offset):
    columns = lax.dynamic_slice_in_dim(left_rows, offset, shard_piece.shape[0], 1)
    return running + jnp.dot(columns, shard_piece, preferred_element_type=jnp.float32)


def project_rows(left_rows, shard_piece, offset):
    return jnp.dot(left_rows, shard_piece, preferred_element_type=jnp.float32)


def shards(
    tokens, norm_gain, val_weight, gate_weight, conv_taps, conv_bias, ln_gain, ln_shift, out_weight
):
    stream = tokens
    num_seqs = tokens.shape[0]
    local_len = tokens.shape[1]
    chan_width = val_weight.shape[2]
    all_channels = chan_width * lax.axis_size("tp")
    half_width = conv_taps.shape[1] // 2
    for layer_idx in range(LAYERS):
        gathered = lax.all_gather(stream, "tp", axis=2, tiled=True)
        widened = gathered.astype(jnp.float32)
        scaled = widened * lax.rsqrt(jnp.mean(widened * widened, axis=-1, keepdims=True) + epsilon)
        normed = (scaled * norm_gain[layer_idx]).astype(jnp.bfloat16)
        tok_rows = normed.reshape(-1, normed.shape[2])
        zeroed = jnp.zeros((tok_rows.shape[0], chan_width), jnp.float32)
        values = over_all(val_weight[layer_idx], "sp", 0, partial(add_rows, tok_rows), zeroed)
        gates = over_all(gate_weight[layer_idx], "sp", 0, partial(add_rows, tok_rows), zeroed)
        gated = (
            (values * jax.nn.sigmoid(gates))
            .astype(jnp.bfloat16)
            .reshape(num_seqs, local_len, chan_width)
        )
        padded = with_halo(gated, (("sp", 1),), half_width, False)
        convolved = (
            depthwise(padded.astype(jnp.float32), conv_taps[layer_idx], local_len)
            + conv_bias[layer_idx]
        )
        first_sum, second_sum = lax.psum(
            (jnp.sum(convolved, axis=-1), jnp.sum(convolved * convolved, axis=-1)), "tp"
        )
        mean_val = (first_sum / all_channels)[..., None]
        spread = (second_sum / all_channels)[..., None] - mean_val * mean_val
        centered = convolved - mean_val
        normalized = (
            centered * lax.rsqrt(spread + epsilon) * ln_gain[layer_idx] + ln_shift[layer_idx]
        )
        activated = jax.nn.silu(normalized).astype(jnp.bfloat16).reshape(-1, chan_width)
        partial_terms = over_all_2(out_weight[layer_idx], "sp", 1, partial(project_rows, activated))
        full_width = partial_terms.shape[1]
        summed = lax.psum_scatter(
            partial_terms.reshape(num_seqs, local_len, full_width).astype(jnp.bfloat16),
            "tp",
            scatter_dimension=2,
            tiled=True,
        ).astype(jnp.float32)
        stream = (stream.astype(jnp.float32) + summed).astype(jnp.bfloat16)
    return stream


def solution(mesh):
    placed = (
        P(None, "sp", "tp"),
        P(),
        P(None, "sp", "tp"),
        P(None, "sp", "tp"),
        P(None, None, "tp"),
        P(None, "tp"),
        P(None, "tp"),
        P(None, "tp"),
        P(None, "tp", "sp"),
    )
    return jax.shard_map(
        shards, mesh=mesh, in_specs=placed, out_specs=P(None, "sp", "tp"), check_vma=False
    )
```

profile of v0, /device:TPU:0, one launch (start us, length us, event | category | flops | bytes accessed | tf_op | source)
XLA Modules:
  0.0 475.9 jit_solution(14715837289468333107)
XLA Ops:
  6.5 0.9 fusion.211
  7.4 8.9 %all_gather.48 = bf16[4,64,1024]{2,1,0:T(8,128)(2,1)S(1)} all-gather(bf16[4,64,256]{2,1,0:T(8,128)(2,1)} %param.9), channel_id=1, replica_groups=mesh['sp'=8,'tp'=4] {'tp'}, dimensions={2}, use_global_device_ids=true | all-gather | bytes 655360 | tf_op jit(solution)/shard_map/all_gather | solution.py:59
  16.3 0.2 fusion.20
  16.5 0.7 copy-done.1
  17.2 31.4 %all-gather = bf16[1,1024,128]{2,1,0:T(8,128)(2,1)S(1)} all-gather(bf16[1,128,128]{2,1,0:T(8,128)(2,1)S(1)} %get-tuple-element.31), channel_id=2, replica_groups=mesh['sp'=8,'tp'=4] {'sp'}, dimensions={1}, use_global_device_ids=true | all-gather | bytes 294912 | tf_op jit(solution)/shard_map/all_gather | solution.py:12
  48.6 30.7 %all-gather.1 = bf16[1,1024,128]{2,1,0:T(8,128)(2,1)S(1)} all-gather(bf16[1,128,128]{2,1,0:T(8,128)(2,1)S(1)} %get-tuple-element.27), channel_id=3, replica_groups=mesh['sp'=8,'tp'=4] {'sp'}, dimensions={1}, use_global_device_ids=true | all-gather | bytes 294912 | tf_op jit(solution)/shard_map/all_gather | solution.py:12
  79.4 0.2 fusion.22
  79.5 0.3 fusion.46
  79.9 0.3 fusion.16
  80.2 3.4 collective-permute-start
  83.6 1.3 collective-permute-start.1
  85.0 0.7 copy-done.5
  85.7 0.6 copy-done.6
  86.4 27.0 %all-gather.2 = bf16[1,128,1024]{2,1,0:T(8,128)(2,1)S(1)} all-gather(bf16[1,128,128]{2,1,0:T(8,128)(2,1)S(1)} %get-tuple-element.33), channel_id=4, replica_groups=mesh['sp'=8,'tp'=4] {'sp'}, dimensions={2}, use_global_device_ids=true | all-gather | bytes 294912 | tf_op jit(solution)/shard_map/all_gather | solution.py:30
  113.4 0.6 fusion.199
  114.0 5.7 %all-reduce.3 = (f32[4,64]{1,0:T(4,128)S(1)}, f32[4,64]{1,0:T(4,128)S(1)}) all-reduce(f32[4,64]{1,0:T(4,128)S(1)} %get-tuple-element.12, f32[4,64]{1,0:T(4,128)S(1)} %get-tuple-element.11), channel_id=1, replica_groups=mesh['sp'=8,'tp'=4] {'tp'}, use_global_device_ids=true, to_apply=%region_4.0 | all-reduce | flops 512 | bytes 4096 | tf_op jit(solution)/shard_map/psum | solution.py:77
  119.7 1.2 convolution_convert_fusion.3
  120.9 0.0 reduce-scatter.7.cloned.1.call-start
  120.9 30.8 %all-gather.3 = bf16[1,1024,128]{2,1,0:T(8,128)(2,1)S(1)} all-gather(bf16[1,128,128]{2,1,0:T(8,128)(2,1)S(1)} %get-tuple-element.30), channel_id=5, replica_groups=mesh['sp'=8,'tp'=4] {'sp'}, dimensions={1}, use_global_device_ids=true | all-gather | bytes 294912 | tf_op jit(solution)/shard_map/all_gather | solution.py:12
  151.7 31.0 %all-gather.4 = bf16[1,1024,128]{2,1,0:T(8,128)(2,1)S(1)} all-gather(bf16[1,128,128]{2,1,0:T(8,128)(2,1)S(1)} %get-tuple-element.26), channel_id=6, replica_groups=mesh['sp'=8,'tp'=4] {'sp'}, dimensions={1}, use_global_device_ids=true | all-gather | bytes 294912 | tf_op jit(solution)/shard_map/all_gather | solution.py:12
  182.7 0.9 add_convert_fusion.3
  183.6 6.8 %all_gather.52 = bf16[4,64,1024]{2,1,0:T(8,128)(2,1)S(1)} all-gather(bf16[4,64,256]{2,1,0:T(8,128)(2,1)S(1)} %add_convert_fusion.3), channel_id=1, replica_groups=mesh['sp'=8,'tp'=4] {'tp'}, dimensions={2}, use_global_device_ids=true | all-gather | bytes 655360 | tf_op jit(solution)/shard_map/all_gather | solution.py:59
  190.4 0.2 fusion.23
  190.6 0.2 fusion.25
  190.8 0.3 fusion.42
  191.1 0.3 fusion.17
  191.4 2.4 collective-permute-start.2
  193.8 1.3 collective-permute-start.3
  195.1 27.1 %all-gather.5 = bf16[1,128,1024]{2,1,0:T(8,128)(2,1)S(1)} all-gather(bf16[1,128,128]{2,1,0:T(8,128)(2,1)S(1)} %get-tuple-element.34), channel_id=7, replica_groups=mesh['sp'=8,'tp'=4] {'sp'}, dimensions={2}, use_global_device_ids=true | all-gather | bytes 294912 | tf_op jit(solution)/shard_map/all_gather | solution.py:30
  222.2 0.6 fusion.198
  222.8 5.7 %all-reduce.2 = (f32[4,64]{1,0:T(4,128)S(1)}, f32[4,64]{1,0:T(4,128)S(1)}) all-reduce(f32[4,64]{1,0:T(4,128)S(1)} %get-tuple-element.10, f32[4,64]{1,0:T(4,128)S(1)} %get-tuple-element.9), channel_id=1, replica_groups=mesh['sp'=8,'tp'=4] {'tp'}, use_global_device_ids=true, to_apply=%region_10.11 | all-reduce | flops 512 | bytes 4096 | tf_op jit(solution)/shard_map/psum | solution.py:77
  228.5 1.2 convolution_convert_fusion.2
  229.7 0.0 reduce-scatter.9.cloned.1.call-start
  229.7 30.8 %all-gather.6 = bf16[1,1024,128]{2,1,0:T(8,128)(2,1)S(1)} all-gather(bf16[1,128,128]{2,1,0:T(8,128)(2,1)S(1)} %get-tuple-element.32), channel_id=8, replica_groups=mesh['sp'=8,'tp'=4] {'sp'}, dimensions={1}, use_global_device_ids=true | all-gather | bytes 294912 | tf_op jit(solution)/shard_map/all_gather | solution.py:12
  260.5 30.7 %all-gather.7 = bf16[1,1024,128]{2,1,0:T(8,128)(2,1)S(1)} all-gather(bf16[1,128,128]{2,1,0:T(8,128)(2,1)S(1)} %get-tuple-element.28), channel_id=9, replica_groups=mesh['sp'=8,'tp'=4] {'sp'}, dimensions={1}, use_global_device_ids=true | all-gather | bytes 294912 | tf_op jit(solution)/shard_map/all_gather | solution.py:12
  291.3 0.9 add_convert_fusion.2
  292.2 6.6 %all_gather.56 = bf16[4,64,1024]{2,1,0:T(8,128)(2,1)S(1)} all-gather(bf16[4,64,256]{2,1,0:T(8,128)(2,1)S(1)} %add_convert_fusion.2), channel_id=1, replica_groups=mesh['sp'=8,'tp'=4] {'tp'}, dimensions={2}, use_global_device_ids=true | all-gather | bytes 655360 | tf_op jit(solution)/shard_map/all_gather | solution.py:59
  298.8 0.2 fusion.26
  299.0 0.2 fusion.28
  299.2 0.3 fusion.38
  299.5 0.3 fusion.18
  299.8 2.5 collective-permute-start.4
  302.3 1.3 collective-permute-start.5
  303.6 27.1 %all-gather.8 = bf16[1,128,1024]{2,1,0:T(8,128)(2,1)S(1)} all-gather(bf16[1,128,128]{2,1,0:T(8,128)(2,1)S(1)} %get-tuple-element.36), channel_id=10, replica_groups=mesh['sp'=8,'tp'=4] {'sp'}, dimensions={2}, use_global_device_ids=true | all-gather | bytes 294912 | tf_op jit(solution)/shard_map/all_gather | solution.py:30
  330.7 0.6 fusion.197
  331.3 5.7 %all-reduce.1 = (f32[4,64]{1,0:T(4,128)S(1)}, f32[4,64]{1,0:T(4,128)S(1)}) all-reduce(f32[4,64]{1,0:T(4,128)S(1)} %get-tuple-element.8, f32[4,64]{1,0:T(4,128)S(1)} %get-tuple-element.7), channel_id=1, replica_groups=mesh['sp'=8,'tp'=4] {'tp'}, use_global_device_ids=true, to_apply=%region_16.17 | all-reduce | flops 512 | bytes 4096 | tf_op jit(solution)/shard_map/psum | solution.py:77
  336.9 1.2 convolution_convert_fusion.1
  338.1 0.0 reduce-scatter.11.cloned.1.call-start
  338.2 30.8 %all-gather.9 = bf16[1,1024,128]{2,1,0:T(8,128)(2,1)S(1)} all-gather(bf16[1,128,128]{2,1,0:T(8,128)(2,1)S(1)} %get-tuple-element.29), channel_id=11, replica_groups=mesh['sp'=8,'tp'=4] {'sp'}, dimensions={1}, use_global_device_ids=true | all-gather | bytes 294912 | tf_op jit(solution)/shard_map/all_gather | solution.py:12
  368.9 30.7 %all-gather.10 = bf16[1,1024,128]{2,1,0:T(8,128)(2,1)S(1)} all-gather(bf16[1,128,128]{2,1,0:T(8,128)(2,1)S(1)} %get-tuple-element.25), channel_id=12, replica_groups=mesh['sp'=8,'tp'=4] {'sp'}, dimensions={1}, use_global_device_ids=true | all-gather | bytes 294912 | tf_op jit(solution)/shard_map/all_gather | solution.py:12
  399.7 0.9 add_convert_fusion.1
  400.6 6.8 %all_gather.60 = bf16[4,64,1024]{2,1,0:T(8,128)(2,1)S(1)} all-gather(bf16[4,64,256]{2,1,0:T(8,128)(2,1)S(1)} %add_convert_fusion.1), channel_id=1, replica_groups=mesh['sp'=8,'tp'=4] {'tp'}, dimensions={2}, use_global_device_ids=true | all-gather | bytes 655360 | tf_op jit(solution)/shard_map/all_gather | solution.py:59
  407.4 0.2 fusion.29
  407.6 0.2 fusion.31
  407.8 0.3 fusion.34
  408.1 0.3 fusion.19
  408.4 2.5 collective-permute-start.6
  410.9 1.3 collective-permute-start.7
  412.2 27.1 %all-gather.11 = bf16[1,128,1024]{2,1,0:T(8,128)(2,1)S(1)} all-gather(bf16[1,128,128]{2,1,0:T(8,128)(2,1)S(1)} %get-tuple-element.35), channel_id=13, replica_groups=mesh['sp'=8,'tp'=4] {'sp'}, dimensions={2}, use_global_device_ids=true | all-gather | bytes 294912 | tf_op jit(solution)/shard_map/all_gather | solution.py:30
  439.3 0.6 fusion.196
  439.8 5.7 %all-reduce = (f32[4,64]{1,0:T(4,128)S(1)}, f32[4,64]{1,0:T(4,128)S(1)}) all-reduce(f32[4,64]{1,0:T(4,128)S(1)} %get-tuple-element.6, f32[4,64]{1,0:T(4,128)S(1)} %get-tuple-element.5), channel_id=1, replica_groups=mesh['sp'=8,'tp'=4] {'tp'}, use_global_device_ids=true, to_apply=%region_22.23 | all-reduce | flops 512 | bytes 4096 | tf_op jit(solution)/shard_map/psum | solution.py:77
  445.5 1.2 convolution_convert_fusion
  446.7 21.1 %reduce-scatter.11.cloned.1.call-done = bf16[4,64,256]{2,1,0:T(8,128)(2,1)} async-done(((bf16[4,64,1024]{2,1,0:T(8,128)(2,1)}), bf16[4,64,256]{2,1,0:T(8,128)(2,1)}) %reduce-scatter.11.cloned.1.call-update) | async-done | bytes 131088 | tf_op jit(solution)/shard_map/reduce_scatter | solution.py:89
  467.7 1.6 add_convert_fusion
  (57 shorter events, 0.5 us)
Async XLA Ops:
  6.5 176.1 %reduce-scatter.5.cloned.1.call-start = ((), (), s32[]{:S(2)}) async-start(), calls=%async_computation.4 | async-start | bytes 655360 | tf_op jit(solution)/shard_map/reduce_scatter | solution.py:89
  16.3 0.9 copy-start.1
  17.2 31.4 %copy-start.2 = (bf16[4,128,128]{2,1,0:T(8,128)(2,1)S(1)}, bf16[4,128,128]{2,1,0:T(8,128)(2,1)}, u32[]{:S(2)}) copy-start(bf16[4,128,128]{2,1,0:T(8,128)(2,1)} %param.12) | copy-start | bytes 393220
  79.8 5.8 %copy-start.3 = (bf16[4,128,128]{2,1,0:T(8,128)(2,1)S(1)}, bf16[4,128,128]{2,1,0:T(8,128)(2,1)}, u32[]{:S(2)}) copy-start(bf16[4,128,128]{2,1,0:T(8,128)(2,1)} %param.17) | copy-start | bytes 393220
  80.2 4.8 copy-start.4
  80.2 33.2 %collective-permute-start = (bf16[4,15,128]{2,1,0:T(8,128)(2,1)S(1)}, bf16[4,15,128]{2,1,0:T(8,128)(2,1)S(1)}, u32[]{:S(2)}, u32[]{:S(2)}) collective-permute-start(bf16[4,15,128]{2,1,0:T(8,128)(2,1)S(1)} %get-tuple-element.43), channel_id=1, source_target_pairs={{0,4},{4,8},{8,12},{12,16},{16,20},{20,24},{24,28},{1,5},{5,9},{9,... | collective-permute-start | bytes 46088 | tf_op jit(solution)/shard_map/ppermute | solution.py:23
  83.6 29.8 %collective-permute-start.1 = (bf16[4,15,128]{2,1,0:T(8,128)(2,1)S(1)}, bf16[4,15,128]{2,1,0:T(8,128)(2,1)S(1)}, u32[]{:S(2)}, u32[]{:S(2)}) collective-permute-start(bf16[4,15,128]{2,1,0:T(8,128)(2,1)S(1)} %get-tuple-element.44), channel_id=1, source_target_pairs={{4,0},{8,4},{12,8},{16,12},{20,16},{24,20},{28,24},{5,1},{9,5},{13... | collective-permute-start | bytes 46088 | tf_op jit(solution)/shard_map/ppermute | solution.py:24
  85.0 0.7 copy-start.5
  85.7 0.7 copy-start.6
  85.7 0.7 copy-start.7
  120.9 170.4 %reduce-scatter.7.cloned.1.call-start = ((), (), s32[]{:S(2)}) async-start(), calls=%async_computation.5 | async-start | bytes 655360 | tf_op jit(solution)/shard_map/reduce_scatter | solution.py:89
  151.7 31.0 %copy-start = (bf16[4,64,256]{2,1,0:T(8,128)(2,1)S(1)}, bf16[4,64,256]{2,1,0:T(8,128)(2,1)}, u32[]{:S(2)}) copy-start(bf16[4,64,256]{2,1,0:T(8,128)(2,1)} %param.9) | copy-start | bytes 393220
  191.4 30.8 %collective-permute-start.2 = (bf16[4,15,128]{2,1,0:T(8,128)(2,1)S(1)}, bf16[4,15,128]{2,1,0:T(8,128)(2,1)S(1)}, u32[]{:S(2)}, u32[]{:S(2)}) collective-permute-start(bf16[4,15,128]{2,1,0:T(8,128)(2,1)S(1)} %get-tuple-element.41), channel_id=1, source_target_pairs={{0,4},{4,8},{8,12},{12,16},{16,20},{20,24},{24,28},{1,5},{5,9},{9,... | collective-permute-start | bytes 46088 | tf_op jit(solution)/shard_map/ppermute | solution.py:23
  193.8 28.4 %collective-permute-start.3 = (bf16[4,15,128]{2,1,0:T(8,128)(2,1)S(1)}, bf16[4,15,128]{2,1,0:T(8,128)(2,1)S(1)}, u32[]{:S(2)}, u32[]{:S(2)}) collective-permute-start(bf16[4,15,128]{2,1,0:T(8,128)(2,1)S(1)} %get-tuple-element.42), channel_id=1, source_target_pairs={{4,0},{8,4},{12,8},{16,12},{20,16},{24,20},{28,24},{5,1},{9,5},{13... | collective-permute-start | bytes 46088 | tf_op jit(solution)/shard_map/ppermute | solution.py:24
  229.7 170.0 %reduce-scatter.9.cloned.1.call-start = ((), (), s32[]{:S(2)}) async-start(), calls=%async_computation.6 | async-start | bytes 655360 | tf_op jit(solution)/shard_map/reduce_scatter | solution.py:89
  299.8 30.8 %collective-permute-start.4 = (bf16[4,15,128]{2,1,0:T(8,128)(2,1)S(1)}, bf16[4,15,128]{2,1,0:T(8,128)(2,1)S(1)}, u32[]{:S(2)}, u32[]{:S(2)}) collective-permute-start(bf16[4,15,128]{2,1,0:T(8,128)(2,1)S(1)} %get-tuple-element.39), channel_id=1, source_target_pairs={{0,4},{4,8},{8,12},{12,16},{16,20},{20,24},{24,28},{1,5},{5,9},{9,... | collective-permute-start | bytes 46088 | tf_op jit(solution)/shard_map/ppermute | solution.py:23
  302.3 28.4 %collective-permute-start.5 = (bf16[4,15,128]{2,1,0:T(8,128)(2,1)S(1)}, bf16[4,15,128]{2,1,0:T(8,128)(2,1)S(1)}, u32[]{:S(2)}, u32[]{:S(2)}) collective-permute-start(bf16[4,15,128]{2,1,0:T(8,128)(2,1)S(1)} %get-tuple-element.40), channel_id=1, source_target_pairs={{4,0},{8,4},{12,8},{16,12},{20,16},{24,20},{28,24},{5,1},{9,5},{13... | collective-permute-start | bytes 46088 | tf_op jit(solution)/shard_map/ppermute | solution.py:24
  338.1 129.6 %reduce-scatter.11.cloned.1.call-start = ((), (), s32[]{:S(2)}) async-start(), calls=%async_computation.7 | async-start | bytes 655360 | tf_op jit(solution)/shard_map/reduce_scatter | solution.py:89
  408.4 30.8 %collective-permute-start.6 = (bf16[4,15,128]{2,1,0:T(8,128)(2,1)S(1)}, bf16[4,15,128]{2,1,0:T(8,128)(2,1)S(1)}, u32[]{:S(2)}, u32[]{:S(2)}) collective-permute-start(bf16[4,15,128]{2,1,0:T(8,128)(2,1)S(1)} %get-tuple-element.37), channel_id=1, source_target_pairs={{0,4},{4,8},{8,12},{12,16},{16,20},{20,24},{24,28},{1,5},{5,9},{9,... | collective-permute-start | bytes 46088 | tf_op jit(solution)/shard_map/ppermute | solution.py:23
  410.9 28.4 %collective-permute-start.7 = (bf16[4,15,128]{2,1,0:T(8,128)(2,1)S(1)}, bf16[4,15,128]{2,1,0:T(8,128)(2,1)S(1)}, u32[]{:S(2)}, u32[]{:S(2)}) collective-permute-start(bf16[4,15,128]{2,1,0:T(8,128)(2,1)S(1)} %get-tuple-element.38), channel_id=1, source_target_pairs={{4,0},{8,4},{12,8},{16,12},{20,16},{24,20},{28,24},{5,1},{9,5},{13... | collective-permute-start | bytes 46088 | tf_op jit(solution)/shard_map/ppermute | solution.py:24
Sparse Core Ops, SparseCore 0:
  121.0 21.0 reduce-scatter.4
  229.8 20.8 reduce-scatter.6
  338.2 21.0 reduce-scatter.8
  446.8 20.8 reduce-scatter.10
where the time goes:
time: 477 us; the launch traced here: 476 us
  blocking collectives  407 us (85%)
  waiting for transfers between devices  21.2 us (4%)
  starting transfers between devices  16 us (3%)
  between operations  13.5 us (3%)
  other arithmetic  8.32 us (2%)
  matrix products  7 us (1%)
    all_gather x8, blocking collectives, over_all(): lax.all_gather(a, axis, axis=dim, tiled=True)  247 us
    all_gather x4, blocking collectives, over_all_2(): return work(lax.all_gather(shard, axis, axis=dim, tiled=True), jnp.int32(0))  108 us
    all_gather x4, blocking collectives, shards(): gathered = lax.all_gather(stream, 'tp', axis=2, tiled=True)  29 us
    psum x4, blocking collectives, shards(): lax.psum((jnp.sum(convolved, axis=-1), jnp.sum(convolved * convolved, axi...  22.6 us
    reduce_scatter x4, waiting for transfers between devices, shards(): lax.psum_scatter(partial_terms.reshape(num_seqs, local_len, full_width).a...  21.1 us
    ppermute x4, starting transfers between devices, with_halo(): before = lax.ppermute(last, axis, up)  10.8 us
  transfers between devices with their start and end apart: 12, of which 1 were waited for; matrix products, arithmetic and copies ran while one was open for 0% of the time, Pallas kernels for 0%

commit v1 on v0

--- a/solution.py
+++ b/solution.py
@@ -56,7 +56,14 @@
     all_channels = chan_width * lax.axis_size("tp")
     half_width = conv_taps.shape[1] // 2
     for layer_idx in range(LAYERS):
-        gathered = lax.all_gather(stream, "tp", axis=2, tiled=True)
+        ring = [stream]
+        for hop in range(3):
+            ring.append(lax.ppermute(ring[-1], "tp", [(dev, (dev + 1) % 4) for dev in range(4)]))
+        gathered = jnp.roll(
+            jnp.concatenate(ring[::-1], axis=2),
+            (lax.axis_index("tp") + 1) * ring[0].shape[2],
+            axis=2,
+        )
         widened = gathered.astype(jnp.float32)
         scaled = widened * lax.rsqrt(jnp.mean(widened * widened, axis=-1, keepdims=True) + epsilon)
         normed = (scaled * norm_gain[layer_idx]).astype(jnp.bfloat16)

time: 477 us -> 552 us (1.16)
  waiting for transfers between devices: 21.2 us -> 112 us
  blocking collectives: 407 us -> 379 us
  starting transfers between devices: 16 us -> 22.4 us
    reduce_scatter x4, waiting for transfers between devices: 21.1 us -> 83.8 us  [shards(): lax.psum_scatter(partial_terms.reshape(num_seqs, local_len, full_width).a...]
    all_gather x4 -> x0, blocking collectives: 29 us -> none  [shards(): gathered = lax.all_gather(stream, 'tp', axis=2, tiled=True)]
    ppermute x0 -> x12, waiting for transfers between devices: none -> 28.5 us  [shards(): lax.ppermute(ring[-1], 'tp', [(dev, (dev + 1) % 4) for dev in range(4)])]
  transfers between devices with their start and end apart: 12 -> 24, of which waited for: 1 -> 12; matrix products, arithmetic and copies ran while one was open for 0% -> 0% of each run, Pallas kernels for 0% -> 0%
where the time goes in v1:
time: 552 us; the launch traced here: 551 us
  blocking collectives  379 us (69%)
  waiting for transfers between devices  112 us (20%)
  starting transfers between devices  22.4 us (4%)
  between operations  13.5 us (2%)
  other arithmetic  12.5 us (2%)
  matrix products  7.06 us (1%)
    all_gather x8, blocking collectives, over_all(): lax.all_gather(a, axis, axis=dim, tiled=True)  248 us
    all_gather x4, blocking collectives, over_all_2(): return work(lax.all_gather(shard, axis, axis=dim, tiled=True), jnp.int32(0))  108 us
    reduce_scatter x4, waiting for transfers between devices, shards(): lax.psum_scatter(partial_terms.reshape(num_seqs, local_len, full_width).a...  83.8 us
    ppermute x12, waiting for transfers between devices, shards(): lax.ppermute(ring[-1], 'tp', [(dev, (dev + 1) % 4) for dev in range(4)])  28.5 us
    psum x4, blocking collectives, shards(): lax.psum((jnp.sum(convolved, axis=-1), jnp.sum(convolved * convolved, axi...  23.1 us
    ppermute x4, starting transfers between devices, with_halo(): before = lax.ppermute(last, axis, up)  14 us
  transfers between devices with their start and end apart: 24, of which 12 were waited for; matrix products, arithmetic and copies ran while one was open for 0% of the time, Pallas kernels for 0%

profile of v1, /device:TPU:0, one launch (start us, length us, event | category | flops | bytes accessed | tf_op | source)
XLA Modules:
  0.0 551.5 jit_solution(16166686036310801899)
XLA Ops:
  6.5 0.5 collective-permute-start
  7.0 0.9 slice_bitcast_fusion.101
  7.9 0.9 slice_bitcast_fusion.135
  8.8 0.9 fusion.237
  9.8 0.9 copy-done.2
  10.7 0.7 copy-done.6
  11.8 2.4 collective-permute-start.1
  14.2 2.0 collective-permute-done.1
  16.2 31.9 %all-gather = bf16[1,1024,128]{2,1,0:T(8,128)(2,1)S(1)} all-gather(bf16[1,128,128]{2,1,0:T(8,128)(2,1)S(1)} %get-tuple-element.40), channel_id=2, replica_groups=mesh['sp'=8,'tp'=4] {'sp'}, dimensions={1}, use_global_device_ids=true | all-gather | bytes 294912 | tf_op jit(solution)/shard_map/all_gather | solution.py:12
  48.1 30.9 %all-gather.1 = bf16[1,1024,128]{2,1,0:T(8,128)(2,1)S(1)} all-gather(bf16[1,128,128]{2,1,0:T(8,128)(2,1)S(1)} %get-tuple-element.36), channel_id=3, replica_groups=mesh['sp'=8,'tp'=4] {'sp'}, dimensions={1}, use_global_device_ids=true | all-gather | bytes 294912 | tf_op jit(solution)/shard_map/all_gather | solution.py:12
  79.0 1.2 fusion.20
  80.8 0.3 fusion.16
  81.1 3.4 collective-permute-start.3
  84.5 1.3 collective-permute-start.4
  85.8 27.1 %all-gather.2 = bf16[1,128,1024]{2,1,0:T(8,128)(2,1)S(1)} all-gather(bf16[1,128,128]{2,1,0:T(8,128)(2,1)S(1)} %get-tuple-element.42), channel_id=4, replica_groups=mesh['sp'=8,'tp'=4] {'sp'}, dimensions={2}, use_global_device_ids=true | all-gather | bytes 294912 | tf_op jit(solution)/shard_map/all_gather | solution.py:30
  112.9 0.6 fusion.227
  113.5 5.7 %all-reduce.3 = (f32[4,64]{1,0:T(4,128)S(1)}, f32[4,64]{1,0:T(4,128)S(1)}) all-reduce(f32[4,64]{1,0:T(4,128)S(1)} %get-tuple-element.13, f32[4,64]{1,0:T(4,128)S(1)} %get-tuple-element.12), channel_id=1, replica_groups=mesh['sp'=8,'tp'=4] {'tp'}, use_global_device_ids=true, to_apply=%region_4.6 | all-reduce | flops 512 | bytes 4096 | tf_op jit(solution)/shard_map/psum | solution.py:84
  119.2 1.2 convolution_convert_fusion.3
  120.4 21.8 %reduce-scatter.5.cloned.1.call-done = bf16[4,64,256]{2,1,0:T(8,128)(2,1)} async-done(((bf16[4,64,1024]{2,1,0:T(8,128)(2,1)}), bf16[4,64,256]{2,1,0:T(8,128)(2,1)}) %reduce-scatter.5.cloned.1.call-update) | async-done | bytes 131088 | tf_op jit(solution)/shard_map/reduce_scatter | solution.py:96
  142.2 0.9 add_convert_fusion.3
  143.2 4.4 collective-permute-done.5
  147.6 4.4 collective-permute-done.6
  152.0 30.8 %all-gather.3 = bf16[1,1024,128]{2,1,0:T(8,128)(2,1)S(1)} all-gather(bf16[1,128,128]{2,1,0:T(8,128)(2,1)S(1)} %get-tuple-element.39), channel_id=5, replica_groups=mesh['sp'=8,'tp'=4] {'sp'}, dimensions={1}, use_global_device_ids=true | all-gather | bytes 294912 | tf_op jit(solution)/shard_map/all_gather | solution.py:12
  182.8 30.8 %all-gather.4 = bf16[1,1024,128]{2,1,0:T(8,128)(2,1)S(1)} all-gather(bf16[1,128,128]{2,1,0:T(8,128)(2,1)S(1)} %get-tuple-element.35), channel_id=6, replica_groups=mesh['sp'=8,'tp'=4] {'sp'}, dimensions={1}, use_global_device_ids=true | all-gather | bytes 294912 | tf_op jit(solution)/shard_map/all_gather | solution.py:12
  213.6 1.2 fusion.23
  215.0 0.3 fusion.70
  215.3 0.3 fusion.17
  215.7 3.5 collective-permute-start.8
  219.2 1.3 collective-permute-start.9
  220.5 27.1 %all-gather.5 = bf16[1,128,1024]{2,1,0:T(8,128)(2,1)S(1)} all-gather(bf16[1,128,128]{2,1,0:T(8,128)(2,1)S(1)} %get-tuple-element.43), channel_id=7, replica_groups=mesh['sp'=8,'tp'=4] {'sp'}, dimensions={2}, use_global_device_ids=true | all-gather | bytes 294912 | tf_op jit(solution)/shard_map/all_gather | solution.py:30
  247.6 0.6 fusion.226
  248.2 5.8 %all-reduce.2 = (f32[4,64]{1,0:T(4,128)S(1)}, f32[4,64]{1,0:T(4,128)S(1)}) all-reduce(f32[4,64]{1,0:T(4,128)S(1)} %get-tuple-element.11, f32[4,64]{1,0:T(4,128)S(1)} %get-tuple-element.10), channel_id=1, replica_groups=mesh['sp'=8,'tp'=4] {'tp'}, use_global_device_ids=true, to_apply=%region_10.12 | all-reduce | flops 512 | bytes 4096 | tf_op jit(solution)/shard_map/psum | solution.py:84
  254.0 1.2 convolution_convert_fusion.2
  255.2 20.6 %reduce-scatter.7.cloned.1.call-done = bf16[4,64,256]{2,1,0:T(8,128)(2,1)} async-done(((bf16[4,64,1024]{2,1,0:T(8,128)(2,1)}), bf16[4,64,256]{2,1,0:T(8,128)(2,1)}) %reduce-scatter.7.cloned.1.call-update) | async-done | bytes 131088 | tf_op jit(solution)/shard_map/reduce_scatter | solution.py:96
  275.9 0.9 add_convert_fusion.2
  276.9 4.4 collective-permute-done.10
  281.3 4.4 collective-permute-done.11
  285.6 30.8 %all-gather.6 = bf16[1,1024,128]{2,1,0:T(8,128)(2,1)S(1)} all-gather(bf16[1,128,128]{2,1,0:T(8,128)(2,1)S(1)} %get-tuple-element.41), channel_id=8, replica_groups=mesh['sp'=8,'tp'=4] {'sp'}, dimensions={1}, use_global_device_ids=true | all-gather | bytes 294912 | tf_op jit(solution)/shard_map/all_gather | solution.py:12
  316.4 30.8 %all-gather.7 = bf16[1,1024,128]{2,1,0:T(8,128)(2,1)S(1)} all-gather(bf16[1,128,128]{2,1,0:T(8,128)(2,1)S(1)} %get-tuple-element.37), channel_id=9, replica_groups=mesh['sp'=8,'tp'=4] {'sp'}, dimensions={1}, use_global_device_ids=true | all-gather | bytes 294912 | tf_op jit(solution)/shard_map/all_gather | solution.py:12
  347.2 1.2 fusion.26
  348.7 0.3 fusion.66
  348.9 0.3 fusion.18
  349.3 3.5 collective-permute-start.13
  352.8 1.3 collective-permute-start.14
  354.1 27.2 %all-gather.8 = bf16[1,128,1024]{2,1,0:T(8,128)(2,1)S(1)} all-gather(bf16[1,128,128]{2,1,0:T(8,128)(2,1)S(1)} %get-tuple-element.45), channel_id=10, replica_groups=mesh['sp'=8,'tp'=4] {'sp'}, dimensions={2}, use_global_device_ids=true | all-gather | bytes 294912 | tf_op jit(solution)/shard_map/all_gather | solution.py:30
  381.4 0.6 fusion.225
  381.9 5.9 %all-reduce.1 = (f32[4,64]{1,0:T(4,128)S(1)}, f32[4,64]{1,0:T(4,128)S(1)}) all-reduce(f32[4,64]{1,0:T(4,128)S(1)} %get-tuple-element.9, f32[4,64]{1,0:T(4,128)S(1)} %get-tuple-element.8), channel_id=1, replica_groups=mesh['sp'=8,'tp'=4] {'tp'}, use_global_device_ids=true, to_apply=%region_16.18 | all-reduce | flops 512 | bytes 4096 | tf_op jit(solution)/shard_map/psum | solution.py:84
  387.8 1.2 convolution_convert_fusion.1
  389.1 20.6 %reduce-scatter.9.cloned.1.call-done = bf16[4,64,256]{2,1,0:T(8,128)(2,1)} async-done(((bf16[4,64,1024]{2,1,0:T(8,128)(2,1)}), bf16[4,64,256]{2,1,0:T(8,128)(2,1)}) %reduce-scatter.9.cloned.1.call-update) | async-done | bytes 131088 | tf_op jit(solution)/shard_map/reduce_scatter | solution.py:96
  409.7 0.9 add_convert_fusion.1
  410.7 4.4 collective-permute-done.15
  415.1 4.4 collective-permute-done.16
  419.5 30.8 %all-gather.9 = bf16[1,1024,128]{2,1,0:T(8,128)(2,1)S(1)} all-gather(bf16[1,128,128]{2,1,0:T(8,128)(2,1)S(1)} %get-tuple-element.38), channel_id=11, replica_groups=mesh['sp'=8,'tp'=4] {'sp'}, dimensions={1}, use_global_device_ids=true | all-gather | bytes 294912 | tf_op jit(solution)/shard_map/all_gather | solution.py:12
  450.3 30.8 %all-gather.10 = bf16[1,1024,128]{2,1,0:T(8,128)(2,1)S(1)} all-gather(bf16[1,128,128]{2,1,0:T(8,128)(2,1)S(1)} %get-tuple-element.34), channel_id=12, replica_groups=mesh['sp'=8,'tp'=4] {'sp'}, dimensions={1}, use_global_device_ids=true | all-gather | bytes 294912 | tf_op jit(solution)/shard_map/all_gather | solution.py:12
  481.1 1.2 fusion.29
  482.8 0.3 fusion.19
  483.1 3.5 collective-permute-start.18
  486.6 1.3 collective-permute-start.19
  487.9 27.1 %all-gather.11 = bf16[1,128,1024]{2,1,0:T(8,128)(2,1)S(1)} all-gather(bf16[1,128,128]{2,1,0:T(8,128)(2,1)S(1)} %get-tuple-element.44), channel_id=13, replica_groups=mesh['sp'=8,'tp'=4] {'sp'}, dimensions={2}, use_global_device_ids=true | all-gather | bytes 294912 | tf_op jit(solution)/shard_map/all_gather | solution.py:30
  515.0 0.6 fusion.224
  515.6 5.8 %all-reduce = (f32[4,64]{1,0:T(4,128)S(1)}, f32[4,64]{1,0:T(4,128)S(1)}) all-reduce(f32[4,64]{1,0:T(4,128)S(1)} %get-tuple-element.7, f32[4,64]{1,0:T(4,128)S(1)} %get-tuple-element.6), channel_id=1, replica_groups=mesh['sp'=8,'tp'=4] {'tp'}, use_global_device_ids=true, to_apply=%region_22.24 | all-reduce | flops 512 | bytes 4096 | tf_op jit(solution)/shard_map/psum | solution.py:84
  521.4 1.2 convolution_convert_fusion
  522.6 20.7 %reduce-scatter.11.cloned.1.call-done = bf16[4,64,256]{2,1,0:T(8,128)(2,1)} async-done(((bf16[4,64,1024]{2,1,0:T(8,128)(2,1)}), bf16[4,64,256]{2,1,0:T(8,128)(2,1)}) %reduce-scatter.11.cloned.1.call-update) | async-done | bytes 131088 | tf_op jit(solution)/shard_map/reduce_scatter | solution.py:96
  543.3 1.6 add_convert_fusion
  (77 shorter events, 2.6 us)
Async XLA Ops:
  6.5 2.2 copy-start.4
  6.5 135.7 %reduce-scatter.5.cloned.1.call-start = ((), (), s32[]{:S(2)}) async-start(), calls=%async_computation.4 | async-start | bytes 655360 | tf_op jit(solution)/shard_map/reduce_scatter | solution.py:96
  6.5 5.3 collective-permute-start
  8.8 1.0 copy-start.1
  9.8 0.9 copy-start.2
  10.7 0.7 copy-start.6
  10.7 0.7 copy-start.7
  10.7 0.9 copy-start.3
  11.6 2.7 copy-start.5
  11.8 4.4 collective-permute-start.1
  16.2 62.8 %collective-permute-start.2 = (bf16[4,64,256]{2,1,0:T(8,128)(2,1)S(1)}, bf16[4,64,256]{2,1,0:T(8,128)(2,1)S(1)}, u32[]{:S(2)}, u32[]{:S(2)}) collective-permute-start(bf16[4,64,256]{2,1,0:T(8,128)(2,1)S(1)} %collective-permute-done.1), channel_id=1, source_target_pairs={{0,1},{1,2},{2,3},{3,0},{4,5},{5,6},{6,7},{7,4},{8,9},{9,10},{10,1... | collective-permute-start | bytes 393224 | tf_op jit(solution)/shard_map/ppermute | solution.py:61
  48.1 30.9 %copy-start = (bf16[4,64,256]{2,1,0:T(8,128)(2,1)S(1)}, bf16[4,64,256]{2,1,0:T(8,128)(2,1)}, u32[]{:S(2)}) copy-start(bf16[4,64,256]{2,1,0:T(8,128)(2,1)} %param.11) | copy-start | bytes 393220
  81.1 31.8 %collective-permute-start.3 = (bf16[4,15,128]{2,1,0:T(8,128)(2,1)S(1)}, bf16[4,15,128]{2,1,0:T(8,128)(2,1)S(1)}, u32[]{:S(2)}, u32[]{:S(2)}) collective-permute-start(bf16[4,15,128]{2,1,0:T(8,128)(2,1)S(1)} %get-tuple-element.52), channel_id=1, source_target_pairs={{0,4},{4,8},{8,12},{12,16},{16,20},{20,24},{24,28},{1,5},{5,9},{9,... | collective-permute-start | bytes 46088 | tf_op jit(solution)/shard_map/ppermute | solution.py:23
  84.5 28.4 %collective-permute-start.4 = (bf16[4,15,128]{2,1,0:T(8,128)(2,1)S(1)}, bf16[4,15,128]{2,1,0:T(8,128)(2,1)S(1)}, u32[]{:S(2)}, u32[]{:S(2)}) collective-permute-start(bf16[4,15,128]{2,1,0:T(8,128)(2,1)S(1)} %get-tuple-element.53), channel_id=1, source_target_pairs={{4,0},{8,4},{12,8},{16,12},{20,16},{24,20},{28,24},{5,1},{9,5},{13... | collective-permute-start | bytes 46088 | tf_op jit(solution)/shard_map/ppermute | solution.py:24
  120.3 155.5 %reduce-scatter.7.cloned.1.call-start = ((), (), s32[]{:S(2)}) async-start(), calls=%async_computation.5 | async-start | bytes 655360 | tf_op jit(solution)/shard_map/reduce_scatter | solution.py:96
  143.2 4.4 collective-permute-start.5
  147.6 4.4 collective-permute-start.6
  152.0 61.6 %collective-permute-start.7 = (bf16[4,64,256]{2,1,0:T(8,128)(2,1)S(1)}, bf16[4,64,256]{2,1,0:T(8,128)(2,1)S(1)}, u32[]{:S(2)}, u32[]{:S(2)}) collective-permute-start(bf16[4,64,256]{2,1,0:T(8,128)(2,1)S(1)} %collective-permute-done.6), channel_id=1, source_target_pairs={{0,1},{1,2},{2,3},{3,0},{4,5},{5,6},{6,7},{7,4},{8,9},{9,10},{10,1... | collective-permute-start | bytes 393224 | tf_op jit(solution)/shard_map/ppermute | solution.py:61
  215.7 31.9 %collective-permute-start.8 = (bf16[4,15,128]{2,1,0:T(8,128)(2,1)S(1)}, bf16[4,15,128]{2,1,0:T(8,128)(2,1)S(1)}, u32[]{:S(2)}, u32[]{:S(2)}) collective-permute-start(bf16[4,15,128]{2,1,0:T(8,128)(2,1)S(1)} %get-tuple-element.50), channel_id=1, source_target_pairs={{0,4},{4,8},{8,12},{12,16},{16,20},{20,24},{24,28},{1,5},{5,9},{9,... | collective-permute-start | bytes 46088 | tf_op jit(solution)/shard_map/ppermute | solution.py:23
  219.2 28.4 %collective-permute-start.9 = (bf16[4,15,128]{2,1,0:T(8,128)(2,1)S(1)}, bf16[4,15,128]{2,1,0:T(8,128)(2,1)S(1)}, u32[]{:S(2)}, u32[]{:S(2)}) collective-permute-start(bf16[4,15,128]{2,1,0:T(8,128)(2,1)S(1)} %get-tuple-element.51), channel_id=1, source_target_pairs={{4,0},{8,4},{12,8},{16,12},{20,16},{24,20},{28,24},{5,1},{9,5},{13... | collective-permute-start | bytes 46088 | tf_op jit(solution)/shard_map/ppermute | solution.py:24
  255.2 154.5 %reduce-scatter.9.cloned.1.call-start = ((), (), s32[]{:S(2)}) async-start(), calls=%async_computation.6 | async-start | bytes 655360 | tf_op jit(solution)/shard_map/reduce_scatter | solution.py:96
  276.8 4.4 collective-permute-start.10
  281.2 4.4 collective-permute-start.11
  285.6 61.6 %collective-permute-start.12 = (bf16[4,64,256]{2,1,0:T(8,128)(2,1)S(1)}, bf16[4,64,256]{2,1,0:T(8,128)(2,1)S(1)}, u32[]{:S(2)}, u32[]{:S(2)}) collective-permute-start(bf16[4,64,256]{2,1,0:T(8,128)(2,1)S(1)} %collective-permute-done.11), channel_id=1, source_target_pairs={{0,1},{1,2},{2,3},{3,0},{4,5},{5,6},{6,7},{7,4},{8,9},{9,10},{10,1... | collective-permute-start | bytes 393224 | tf_op jit(solution)/shard_map/ppermute | solution.py:61
  349.3 32.1 %collective-permute-start.13 = (bf16[4,15,128]{2,1,0:T(8,128)(2,1)S(1)}, bf16[4,15,128]{2,1,0:T(8,128)(2,1)S(1)}, u32[]{:S(2)}, u32[]{:S(2)}) collective-permute-start(bf16[4,15,128]{2,1,0:T(8,128)(2,1)S(1)} %get-tuple-element.48), channel_id=1, source_target_pairs={{0,4},{4,8},{8,12},{12,16},{16,20},{20,24},{24,28},{1,5},{5,9},{9,... | collective-permute-start | bytes 46088 | tf_op jit(solution)/shard_map/ppermute | solution.py:23
  352.8 28.5 %collective-permute-start.14 = (bf16[4,15,128]{2,1,0:T(8,128)(2,1)S(1)}, bf16[4,15,128]{2,1,0:T(8,128)(2,1)S(1)}, u32[]{:S(2)}, u32[]{:S(2)}) collective-permute-start(bf16[4,15,128]{2,1,0:T(8,128)(2,1)S(1)} %get-tuple-element.49), channel_id=1, source_target_pairs={{4,0},{8,4},{12,8},{16,12},{20,16},{24,20},{28,24},{5,1},{9,5},{13... | collective-permute-start | bytes 46088 | tf_op jit(solution)/shard_map/ppermute | solution.py:24
  389.0 154.3 %reduce-scatter.11.cloned.1.call-start = ((), (), s32[]{:S(2)}) async-start(), calls=%async_computation.7 | async-start | bytes 655360 | tf_op jit(solution)/shard_map/reduce_scatter | solution.py:96
  410.6 4.4 collective-permute-start.15
  415.1 4.4 collective-permute-start.16
  419.5 61.6 %collective-permute-start.17 = (bf16[4,64,256]{2,1,0:T(8,128)(2,1)S(1)}, bf16[4,64,256]{2,1,0:T(8,128)(2,1)S(1)}, u32[]{:S(2)}, u32[]{:S(2)}) collective-permute-start(bf16[4,64,256]{2,1,0:T(8,128)(2,1)S(1)} %collective-permute-done.16), channel_id=1, source_target_pairs={{0,1},{1,2},{2,3},{3,0},{4,5},{5,6},{6,7},{7,4},{8,9},{9,10},{10,1... | collective-permute-start | bytes 393224 | tf_op jit(solution)/shard_map/ppermute | solution.py:61
  483.1 31.9 %collective-permute-start.18 = (bf16[4,15,128]{2,1,0:T(8,128)(2,1)S(1)}, bf16[4,15,128]{2,1,0:T(8,128)(2,1)S(1)}, u32[]{:S(2)}, u32[]{:S(2)}) collective-permute-start(bf16[4,15,128]{2,1,0:T(8,128)(2,1)S(1)} %get-tuple-element.46), channel_id=1, source_target_pairs={{0,4},{4,8},{8,12},{12,16},{16,20},{20,24},{24,28},{1,5},{5,9},{9,... | collective-permute-start | bytes 46088 | tf_op jit(solution)/shard_map/ppermute | solution.py:23
  486.6 28.4 %collective-permute-start.19 = (bf16[4,15,128]{2,1,0:T(8,128)(2,1)S(1)}, bf16[4,15,128]{2,1,0:T(8,128)(2,1)S(1)}, u32[]{:S(2)}, u32[]{:S(2)}) collective-permute-start(bf16[4,15,128]{2,1,0:T(8,128)(2,1)S(1)} %get-tuple-element.47), channel_id=1, source_target_pairs={{4,0},{8,4},{12,8},{16,12},{20,16},{24,20},{28,24},{5,1},{9,5},{13... | collective-permute-start | bytes 46088 | tf_op jit(solution)/shard_map/ppermute | solution.py:24
Sparse Core Ops, SparseCore 0:
  120.5 21.7 reduce-scatter.4
  255.3 20.5 reduce-scatter.6
  389.1 20.5 reduce-scatter.8
  522.8 20.5 reduce-scatter.10
